TPU v7x, 32 devices: a whole 2x2x4 slice. The times are simulated.
32 devices in a mesh: ep: 8 (over z, x), tp: 4 (over y, core).
Axes of the slice: x: 2, y: 2, z: 4, core: 2. Of those that a mesh axis runs over, the one named last changes fastest.
Arguments:
- x_mix: bfloat16 [2048, 2048], P('ep'), may hold values from -6 to 6
- mix_gain: float32 [2048], replicated, may hold values from 0.1 to 1.9
- w_query: bfloat16 [2048, 2048], P(None, 'tp'), may hold values from -0.125 to 0.125
- w_key: bfloat16 [2048, 2048], P(None, 'tp'), may hold values from -0.125 to 0.125
- w_value: bfloat16 [2048, 2048], P(None, 'tp'), may hold values from -0.125 to 0.125
- query_gain: float32 [64], replicated, may hold values from 1 to 1.8
- key_gain: float32 [64], replicated, may hold values from 1 to 1.8
- mix_lambda: float32 [16], P('tp'), may hold values from 0.3 to 0.8
- head_gain: float32 [128], replicated, may hold values from 0.1 to 1.9
- w_mix_out: bfloat16 [2048, 2048], P(None, 'tp'), may hold values from -0.125 to 0.125
- x_exp: bfloat16 [1024, 2048], P('ep'), may hold values from -6 to 6
- exp_gain: float32 [2048], replicated, may hold values from 0.1 to 1.9
- routes: int32 [1024, 4], P('ep'), may hold values from 0 to 7, all different within a row; in each aligned block of 128 rows (0 to 127, 128 to 255, ...) at most 96 rows name the same one
- route_weight: float32 [1024, 4], P('ep'), may hold values from 0.1 to 1
- w_gate: bfloat16 [8, 2048, 2048], P('ep', None, 'tp'), may hold values from -0.375 to 0.375
- w_up: bfloat16 [8, 2048, 2048], P('ep', None, 'tp'), may hold values from -0.375 to 0.375
- w_down: bfloat16 [8, 2048, 2048], P('ep', None, 'tp'), may hold values from -0.03125 to 0.03125
Outputs:
- attn_out: bfloat16 [2048, 2048], P('ep', 'tp')
- moe_out: bfloat16 [1024, 2048], P('ep', 'tp')
Inputs may be any that keep to these rules, and one draw needn't show every extreme that they name: `routes`: each row names 4 different experts. In each aligned block of 128 rows (the rows of one index of ep), no expert is named by more than 96 rows, a bound that some block reaches.
All inputs are finite; a program needn't handle non-finite values.
Results may differ from a plain program's by a relative error of at most 0.011.
Values may be sent and summed in bfloat16 or wider, within the bound.
A program may use at most 128 MiB of HBM per device.

v0:
```python
import jax
import jax.numpy as jnp
from jax import lax
from jax.sharding import PartitionSpec as P


def rms_rows(matrix, gain, epsilon):
    wide = matrix.astype(jnp.float32)
    return wide * lax.rsqrt(jnp.mean(wide * wide, axis=-1, keepdims=True) + epsilon) * gain


def slot_ids(chosen_rows, experts, capacity):
    flat_ids = chosen_rows.reshape(-1)
    onehot = (flat_ids[:, None] == lax.iota(jnp.int32, experts)[None, :]).astype(jnp.int32)
    before = jnp.cumsum(onehot, axis=0) - onehot
    position = jnp.sum(before * onehot, axis=1)
    return flat_ids * capacity + position


def attend(
    x_mix, mix_gain, w_query, w_key, w_value, query_gain, key_gain, mix_lambda, head_gain, w_mix_out
):
    row_count = x_mix.shape[0]
    head_size = query_gain.shape[0]
    head_count = w_query.shape[1] // (2 * head_size)
    normed = rms_rows(x_mix, mix_gain, 1e-05).astype(jnp.bfloat16)
    queries = jnp.dot(normed, w_query, preferred_element_type=jnp.float32).reshape(
        row_count, head_count, 2, head_size
    )
    queries = (rms_rows(queries, query_gain, 1e-06) * head_size ** (-0.5)).astype(jnp.bfloat16)
    key_rows = jnp.dot(normed, w_key, preferred_element_type=jnp.float32).reshape(
        row_count, head_count, 2, head_size
    )
    key_rows = (
        rms_rows(key_rows, key_gain, 1e-06)
        .astype(jnp.bfloat16)
        .reshape(row_count, head_count * 2 * head_size)
    )
    values = jnp.dot(normed, w_value, preferred_element_type=jnp.float32).astype(jnp.bfloat16)
    query_pos = lax.axis_index("ep") * row_count + lax.iota(jnp.int32, row_count)
    key_piece = lax.all_gather(key_rows, "ep", axis=0, tiled=True)
    value_piece = lax.all_gather(values, "ep", axis=0, tiled=True)
    piece_rows = key_piece.shape[0]
    key_piece = key_piece.reshape(piece_rows, head_count, 2, head_size)
    value_piece = value_piece.reshape(piece_rows, head_count, 2 * head_size)
    scores = jnp.einsum("qhcd,khcd->cqhk", queries, key_piece, preferred_element_type=jnp.float32)
    key_pos = lax.iota(jnp.int32, piece_rows)
    visible = key_pos[None, :] <= query_pos[:, None]
    weights_exp = jnp.where(visible[None, :, None, :], jnp.exp(scores), 0.0)
    denominator = jnp.sum(weights_exp, axis=-1)
    numerator = jnp.einsum(
        "cqhk,khd->cqhd",
        weights_exp.astype(jnp.bfloat16),
        value_piece,
        preferred_element_type=jnp.float32,
    )
    numerator, denominator = (numerator, denominator)
    head_mix = (
        numerator[0] / denominator[0][..., None]
        - mix_lambda[None, :, None] * numerator[1] / denominator[1][..., None]
    )
    head_rows = (rms_rows(head_mix, head_gain, 1e-05) * 0.8).astype(jnp.bfloat16)
    head_rows = head_rows.reshape(row_count, head_count * 2 * head_size)
    projected = jnp.dot(
        lax.all_gather(head_rows, "tp", axis=1, tiled=True),
        w_mix_out,
        preferred_element_type=jnp.float32,
    )
    return projected.astype(jnp.bfloat16)


def route_experts(x_exp, exp_gain, routes, route_weight, w_gate, w_up, w_down):
    row_count = x_exp.shape[0]
    top_count = routes.shape[1]
    model_width = x_exp.shape[1]
    experts = lax.axis_size("ep")
    capacity = 3 * row_count * top_count // (2 * experts)
    gate_local = w_gate[0]
    up_local = w_up[0]
    down_local = w_down[0]
    local_width = down_local.shape[1]
    normed = rms_rows(x_exp, exp_gain, 1e-05).astype(jnp.bfloat16)
    slot_index = slot_ids(routes, experts, capacity)
    pair_rows = lax.iota(jnp.int32, row_count * top_count) // top_count
    source = jnp.zeros((experts * capacity,), jnp.int32).at[slot_index].set(pair_rows)
    filled = jnp.zeros((experts * capacity,), jnp.bool_).at[slot_index].set(True)
    picked_rows = jnp.where(filled[:, None], normed[source], jnp.zeros((), jnp.bfloat16))
    outgoing = picked_rows.reshape(experts, capacity, model_width)
    incoming = lax.all_to_all(outgoing, "ep", split_axis=0, concat_axis=0, tiled=True)
    item_count = incoming.shape[1]
    flat_rows = incoming.reshape(-1, model_width)
    gate_pre = jnp.dot(flat_rows, gate_local, preferred_element_type=jnp.float32)
    up_pre = jnp.dot(flat_rows, up_local, preferred_element_type=jnp.float32)
    expert_gate_pre = gate_pre
    expert_up_pre = up_pre
    expert_gate_pre = jnp.minimum(expert_gate_pre, 7.0)
    expert_up_pre = jnp.clip(expert_up_pre, -7.0, 7.0)
    hidden = (
        expert_gate_pre * jax.nn.sigmoid(1.702 * expert_gate_pre) * (expert_up_pre + 1.0)
    ).astype(jnp.bfloat16)
    result = jnp.dot(
        lax.all_gather(hidden, "tp", axis=1, tiled=True),
        down_local,
        preferred_element_type=jnp.float32,
    )
    result = result.astype(jnp.bfloat16).reshape(experts, item_count, local_width)
    returned = lax.all_to_all(result, "ep", split_axis=0, concat_axis=0, tiled=True)
    picked = returned.reshape(experts * capacity, local_width)[slot_index]
    picked = picked.reshape(row_count, top_count, local_width).astype(jnp.float32)
    combined = jnp.sum(picked * route_weight[:, :, None], axis=1)
    return combined.astype(jnp.bfloat16)


def body(
    x_mix,
    mix_gain,
    w_query,
    w_key,
    w_value,
    query_gain,
    key_gain,
    mix_lambda,
    head_gain,
    w_mix_out,
    x_exp,
    exp_gain,
    routes,
    route_weight,
    w_gate,
    w_up,
    w_down,
):
    attn_out = attend(
        x_mix,
        mix_gain,
        w_query,
        w_key,
        w_value,
        query_gain,
        key_gain,
        mix_lambda,
        head_gain,
        w_mix_out,
    )
    moe_out = route_experts(x_exp, exp_gain, routes, route_weight, w_gate, w_up, w_down)
    return (attn_out, moe_out)


def solution(mesh):
    return jax.shard_map(
        body,
        mesh=mesh,
        in_specs=(
            P("ep", None),
            P(),
            P(None, "tp"),
            P(None, "tp"),
            P(None, "tp"),
            P(),
            P(),
            P("tp"),
            P(),
            P(None, "tp"),
            P("ep", None),
            P(),
            P("ep", None),
            P("ep", None),
            P("ep", None, "tp"),
            P("ep", None, "tp"),
            P("ep", None, "tp"),
        ),
        out_specs=(P("ep", "tp"), P("ep", "tp")),
        check_vma=False,
    )
```

profile of v0, /device:TPU:0, one launch (start us, length us, event | category | flops | bytes accessed | tf_op | source)
XLA Modules:
  0.0 233.7 jit_solution(14530396072772306226)
XLA Ops:
  7.2 1.6 fusion.4
  8.9 3.5 %fusion.52 = (f32[256,512]{1,0:T(8,128)S(1)}, f32[256,512]{1,0:T(8,128)}) fusion(bf16[2048,512]{1,0:T(8,128)(2,1)} %param.20, bf16[256,2048]{1,0:T(8,128)(2,1)} %param.17, f32[2048]{0:T(1024)} %param.18, f32[256]{0:T(256)S(1)} %add_rsqrt_fusion.3), kind=kOutput, calls=%fused_computation.90 | convolution fusion | flops 539099136 | bytes 4203520 | tf_op jit(solution)/shard_map/dot_general | solution.py:31
  12.7 0.9 mul.194
  13.5 1.2 copy.27
  14.9 1.9 multiply_convert_fusion.2
  17.1 1.1 reduce-window.6
  18.9 2.4 %scatter_custom_fusion.1 = s32[768]{0:T(1024)S(1)} fusion(s32[512]{0:T(512)S(1)} %bitcast.123, s32[512]{0:T(512)S(1)} %add_select_fusion, s32[]{:T(128)} %constant.65.clone.1), kind=kCustom, calls=%fused_computation.76 | custom fusion | bytes 3076 | tf_op jit(solution)/shard_map/scatter | solution.py:85
  21.6 2.4 %scatter_custom_fusion = pred[768]{0:T(1024)(128)(4,1)S(1)} fusion(s32[512]{0:T(512)S(1)} %bitcast.124, pred[512]{0:T(512)(128)(4,1)S(1)} %broadcast.164, pred[]{:T(512)} %constant.25.clone.1), kind=kCustom, calls=%fused_computation.79 | custom fusion | bytes 769 | tf_op jit(solution)/shard_map/scatter | solution.py:86
  24.3 4.3 %gather_fusion = bf16[768,2048]{1,0:T(8,128)(2,1)} fusion(bf16[128,2048]{1,0:T(8,128)(2,1)S(1)} %fusion.25, s32[1024]{0:T(1024)S(1)} %pad_clamp_fusion.1), kind=kCustom, calls=%fused_computation | custom fusion | bytes 6294528 | tf_op jit(solution)/shard_map/gather | solution.py:87
  28.6 3.9 %broadcast_select_fusion = bf16[8,96,2048]{2,1,0:T(8,128)(2,1)} fusion(bf16[8,96,2048]{2,1,0:T(8,128)(2,1)} %bitcast.118, pred[8,96]{1,0:T(8,128)(4,1)S(1)} %broadcast_in_dim.32), kind=kLoop, calls=%fused_computation.9 | loop fusion | flops 1572864 | bytes 6292224 | tf_op jit(solution)/shard_map/jit(_where)/select_n | solution.py:87
  32.5 7.4 %all-to-all-start = ((bf16[8,96,2048]{2,1,0:T(8,128)(2,1)}), bf16[8,96,2048]{2,1,0:T(8,128)(2,1)}, u32[]{:S(2)}, u32[]{:S(2)}) async-start(bf16[8,96,2048]{2,1,0:T(8,128)(2,1)} %broadcast_select_fusion), calls=%async_computation | async-start | bytes 6291456 | tf_op jit(solution)/shard_map/all_to_all | solution.py:89
  40.0 3.0 %convolution_convert_fusion.1 = bf16[256,512]{1,0:T(8,128)(2,1)} fusion(bf16[2048,512]{1,0:T(8,128)(2,1)} %param.21, bf16[256,2048]{1,0:T(8,128)(2,1)S(1)} %copy-done.3, f32[2048]{0:T(1024)S(1)} %copy-done.11, f32[256]{0:T(256)S(1)} %add_rsqrt_fusion.3), kind=kOutput, calls=%fused_computation.30 | convolution fusion | flops 539099136 | bytes 3417088 | tf_op jit(solution)/shard_map/dot_general | solution.py:39
  43.1 93.0 %all-to-all-done = bf16[8,96,2048]{2,1,0:T(8,128)(2,1)} async-done(((bf16[8,96,2048]{2,1,0:T(8,128)(2,1)}), bf16[8,96,2048]{2,1,0:T(8,128)(2,1)}, u32[]{:S(2)}, u32[]{:S(2)}) %all-to-all-start) | async-done | bytes 3145760 | tf_op jit(solution)/shard_map/all_to_all | solution.py:89
  136.1 3.8 %fusion.11 = f32[768,512]{1,0:T(8,128)S(1)} fusion(bf16[768,2048]{1,0:T(8,128)(2,1)} %bitcast.25, bf16[1,2048,512]{2,1,0:T(8,128)(2,1)S(1)} %copy-done), kind=kOutput, calls=%fused_computation.19 | convolution fusion | flops 1610612736 | bytes 6815744 | tf_op jit(solution)/shard_map/dot_general | solution.py:92
  140.0 4.9 %multiply_convert_fusion = bf16[768,512]{1,0:T(8,128)(2,1)} fusion(f32[768,512]{1,0:T(8,128)S(1)} %fusion.11, bf16[768,2048]{1,0:T(8,128)(2,1)} %bitcast.25, bf16[1,2048,512]{2,1,0:T(8,128)(2,1)S(1)} %copy-done.10), kind=kOutput, calls=%fused_computation.24 | convolution fusion | flops 1614544896 | bytes 7602176 | tf_op jit(solution)/shard_map/dot_general | solution.py:93
  145.3 3.5 %multiply_reduce_fusion.1 = (f32[256,4,2]{0,2,1:T(2,128)S(1)}, f32[256,512]{0,1:T(8,128)}) fusion(bf16[2048,512]{1,0:T(8,128)(2,1)} %param.19, bf16[256,2048]{1,0:T(8,128)(2,1)S(1)} %copy-done.3, f32[2048]{0:T(1024)S(1)} %copy-done.11, f32[256]{0:T(256)S(1)} %add_rsqrt_fusion.3), kind=kOutput, calls=%fused_computation.49 | convolution fusion | flops 539228160 | bytes 3687424 | tf_op jit(solution)/shard_map/dot_general | solution.py:27
  148.8 0.3 iota_compare_fusion
  149.1 4.0 %copy.28 = bf16[2048,512]{0,1:T(8,128)(2,1)} copy(bf16[2048,512]{1,0:T(8,128)(2,1)} %all-gather.7.cloned.1.call-done) | data formatting | bytes 4194304 | tf_op jit(solution)/shard_map/all_gather | solution.py:41
  153.1 8.7 %all-gather.5.cloned.1.call-done = bf16[2048,512]{1,0:T(8,128)(2,1)} async-done(((bf16[256,512]{1,0:T(8,128)(2,1)}), bf16[2048,512]{1,0:T(8,128)(2,1)}) %all-gather.5.cloned.1.call-update) | async-done | bytes 2097168 | tf_op jit(solution)/shard_map/all_gather | solution.py:42
  161.9 3.9 %copy.42 = bf16[2048,512]{0,1:T(8,128)(2,1)} copy(bf16[2048,512]{1,0:T(8,128)(2,1)} %all-gather.5.cloned.1.call-done) | data formatting | bytes 4194304 | tf_op jit(solution)/shard_map/reshape | solution.py:45
  165.8 6.7 %fusion = (f32[2,256,4]{1,2,0:T(4,128)S(1)}, bf16[2,256,4,2048]{1,3,2,0:T(8,128)(2,1)S(1)}) fusion(pred[256,2048]{0,1:T(8,128)(4,1)S(1)} %iota_compare_fusion, bf16[2048,4,2,64]{0,3,2,1:T(8,128)(2,1)} %bitcast.120, f32[64]{0:T(128)S(1)} %copy-done.12, f32[256,4,2]{0,2,1:T(2,128)S(1)} %add_rsqrt_fusion, f32[256,512]{0,1:T(8,128)S(1)} %copy-done.13), kind=kOutput, calls=%fused_computation.5 | convolution fusion | flops 549976064 | bytes 11550976 | tf_op jit(solution)/shard_map/qhcd,khcd->cqhk/dot_general | solution.py:46
  172.5 1.3 fusion.20
  174.1 0.9 fusion.33
  175.1 15.4 %all-gather.11.cloned.1.call-done = bf16[768,2048]{1,0:T(8,128)(2,1)} async-done(((bf16[768,512]{1,0:T(8,128)(2,1)}), bf16[768,2048]{1,0:T(8,128)(2,1)}) %all-gather.11.cloned.1.call-update) | async-done | bytes 3145744 | tf_op jit(solution)/shard_map/all_gather | solution.py:102
  190.5 5.2 %fusion.17 = bf16[768,512]{1,0:T(8,128)(2,1)} fusion(bf16[768,2048]{1,0:T(8,128)(2,1)} %all-gather.11.cloned.1.call-done, bf16[1,2048,512]{2,1,0:T(8,128)(2,1)} %param.33), kind=kOutput, calls=%fused_computation.25 | convolution fusion | flops 1611005952 | bytes 6029312 | tf_op jit(solution)/shard_map/dot_general | solution.py:101
  195.7 5.5 %all-to-all-start.1 = ((bf16[8,96,512]{2,1,0:T(8,128)(2,1)}), bf16[8,96,512]{2,1,0:T(8,128)(2,1)S(1)}, u32[]{:S(2)}, u32[]{:S(2)}) async-start(bf16[8,96,512]{2,1,0:T(8,128)(2,1)} %bitcast.122), calls=%async_computation.1 | async-start | bytes 1572864 | tf_op jit(solution)/shard_map/all_to_all | solution.py:107
  201.4 7.9 %all-gather.9.cloned.1.call-done = bf16[256,2048]{0,1:T(8,128)(2,1)} async-done(((bf16[256,512]{0,1:T(8,128)(2,1)}), bf16[256,2048]{0,1:T(8,128)(2,1)}) %all-gather.9.cloned.1.call-update) | async-done | bytes 1048592 | tf_op jit(solution)/shard_map/all_gather | solution.py:65
  209.2 3.3 %convolution_convert_fusion = bf16[256,512]{1,0:T(8,128)(2,1)} fusion(bf16[256,2048]{0,1:T(8,128)(2,1)} %all-gather.9.cloned.1.call-done, bf16[2048,512]{1,0:T(8,128)(2,1)} %param.26), kind=kOutput, calls=%fused_computation.29 | convolution fusion | flops 537001984 | bytes 3407872 | tf_op jit(solution)/shard_map/dot_general | solution.py:64
  212.6 9.2 %all-to-all-done.1 = bf16[8,96,512]{2,1,0:T(8,128)(2,1)S(1)} async-done(((bf16[8,96,512]{2,1,0:T(8,128)(2,1)}), bf16[8,96,512]{2,1,0:T(8,128)(2,1)S(1)}, u32[]{:S(2)}, u32[]{:S(2)}) %all-to-all-start.1) | async-done | bytes 786464 | tf_op jit(solution)/shard_map/all_to_all | solution.py:107
  221.8 2.6 %gather_fusion.1 = bf16[512,512]{1,0:T(8,128)(2,1)} fusion(bf16[768,512]{1,0:T(8,128)(2,1)S(1)} %bitcast.117, s32[1024]{0:T(1024)S(1)} %pad_clamp_fusion), kind=kCustom, calls=%fused_computation.1 | custom fusion | bytes 1050624 | tf_op jit(solution)/shard_map/gather | solution.py:108
  224.4 1.4 reshape.170
  225.8 1.4 multiply_reduce_fusion
  (72 shorter events, 2.8 us)
Async XLA Ops:
  7.2 129.0 %copy-start = (bf16[1,2048,512]{2,1,0:T(8,128)(2,1)S(1)}, bf16[1,2048,512]{2,1,0:T(8,128)(2,1)}, u32[]{:S(2)}) copy-start(bf16[1,2048,512]{2,1,0:T(8,128)(2,1)} %param.31) | copy-start | bytes 6291460
  7.2 141.9 %all-gather.7.cloned.1.call-start = ((), (), s32[]{:S(2)}) async-start(), calls=%async_computation.3 | async-start | bytes 2359296 | tf_op jit(solution)/shard_map/all_gather | solution.py:41
  12.4 2.4 %copy-start.8 = (f32[64]{0:T(128)S(1)}, f32[64]{0:T(128)}, u32[]{:S(2)}) copy-start(f32[64]{0:T(128)} %param.23) | copy-start | bytes 772
  12.6 4.2 %copy-start.5 = (s32[128,4]{0,1:T(4,128)S(1)}, s32[128,4]{0,1:T(4,128)}, u32[]{:S(2)}) copy-start(s32[128,4]{0,1:T(4,128)} %param.29) | copy-start | bytes 6148
  12.6 8.8 %copy-start.2 = (bf16[128,2048]{1,0:T(8,128)(2,1)S(1)}, bf16[128,2048]{1,0:T(8,128)(2,1)}, u32[]{:S(2)}) copy-start(bf16[128,2048]{1,0:T(8,128)(2,1)} %param.27) | copy-start | bytes 1572868
  12.7 11.5 %copy-start.4 = (f32[2048]{0:T(1024)S(1)}, f32[2048]{0:T(1024)}, u32[]{:S(2)}) copy-start(f32[2048]{0:T(1024)} %param.28) | copy-start | bytes 24580
  32.5 7.5 %copy-start.3 = (bf16[256,2048]{1,0:T(8,128)(2,1)S(1)}, bf16[256,2048]{1,0:T(8,128)(2,1)}, u32[]{:S(2)}) copy-start(bf16[256,2048]{1,0:T(8,128)(2,1)} %param.17) | copy-start | bytes 3145732
  32.5 7.5 %copy-start.11 = (f32[2048]{0:T(1024)S(1)}, f32[2048]{0:T(1024)}, u32[]{:S(2)}) copy-start(f32[2048]{0:T(1024)} %param.18) | copy-start | bytes 24580
  32.5 103.6 %all-to-all-start = ((bf16[8,96,2048]{2,1,0:T(8,128)(2,1)}), bf16[8,96,2048]{2,1,0:T(8,128)(2,1)}, u32[]{:S(2)}, u32[]{:S(2)}) async-start(bf16[8,96,2048]{2,1,0:T(8,128)(2,1)} %broadcast_select_fusion), calls=%async_computation | async-start | bytes 6291456 | tf_op jit(solution)/shard_map/all_to_all | solution.py:89
  39.9 121.9 %all-gather.5.cloned.1.call-start = ((), (), s32[]{:S(2)}) async-start(), calls=%async_computation.2 | async-start | bytes 2359296 | tf_op jit(solution)/shard_map/all_gather | solution.py:42
  43.1 147.4 %all-gather.11.cloned.1.call-start = ((), (), s32[]{:S(2)}) async-start(), calls=%async_computation.5 | async-start | bytes 3932160 | tf_op jit(solution)/shard_map/all_gather | solution.py:102
  136.1 3.8 %copy-start.10 = (bf16[1,2048,512]{2,1,0:T(8,128)(2,1)S(1)}, bf16[1,2048,512]{2,1,0:T(8,128)(2,1)}, u32[]{:S(2)}) copy-start(bf16[1,2048,512]{2,1,0:T(8,128)(2,1)} %param.32) | copy-start | bytes 6291460
  140.0 5.2 %copy-start.6 = (f32[4]{0:T(128)S(1)}, f32[4]{0:T(128)}, u32[]{:S(2)}) copy-start(f32[4]{0:T(128)} %param.24) | copy-start | bytes 52
  140.0 5.2 %copy-start.9 = (f32[128]{0:T(128)S(1)}, f32[128]{0:T(128)}, u32[]{:S(2)}) copy-start(f32[128]{0:T(128)} %param.25) | copy-start | bytes 1540
  144.9 64.3 %all-gather.9.cloned.1.call-start = ((), (), s32[]{:S(2)}) async-start(), calls=%async_computation.4 | async-start | bytes 1310720 | tf_op jit(solution)/shard_map/all_gather | solution.py:65
  153.1 12.7 %copy-start.12 = (f32[64]{0:T(128)S(1)}, f32[64]{0:T(128)}, u32[]{:S(2)}) copy-start(f32[64]{0:T(128)} %param.22) | copy-start | bytes 772
  153.1 12.7 %copy-start.13 = (f32[256,512]{0,1:T(8,128)S(1)}, f32[256,512]{0,1:T(8,128)}, u32[]{:S(2)}) copy-start(f32[256,512]{0,1:T(8,128)} %get-tuple-element.11) | copy-start | bytes 1572868
  165.8 6.7 %copy-start.1 = (bf16[2048,512]{0,1:T(8,128)(2,1)S(1)}, bf16[2048,512]{0,1:T(8,128)(2,1)}, u32[]{:S(2)}) copy-start(bf16[2048,512]{0,1:T(8,128)(2,1)} %copy.42) | copy-start | bytes 6291460
  175.0 26.2 %copy-start.7 = (f32[128,4]{0,1:T(4,128)S(1)}, f32[128,4]{0,1:T(4,128)}, u32[]{:S(2)}) copy-start(f32[128,4]{0,1:T(4,128)} %param.30) | copy-start | bytes 6148
  195.7 26.1 %all-to-all-start.1 = ((bf16[8,96,512]{2,1,0:T(8,128)(2,1)}), bf16[8,96,512]{2,1,0:T(8,128)(2,1)S(1)}, u32[]{:S(2)}, u32[]{:S(2)}) async-start(bf16[8,96,512]{2,1,0:T(8,128)(2,1)} %bitcast.122), calls=%async_computation.1 | async-start | bytes 1572864 | tf_op jit(solution)/shard_map/all_to_all | solution.py:107
Sparse Core Ops, SparseCore 0:
  16.9 67.8 all-gather.6
  87.5 74.3 all-gather.4
  163.4 27.0 all-gather.10
  192.5 16.6 all-gather.8
where the time goes:
time: 234 us
  waiting for transfers between devices  134 us (57%)
  matrix products  35.2 us (15%)
  local copies, waits for them, and re-layouts  24.7 us (11%)
  between operations  14.1 us (6%)
  starting transfers between devices  13.3 us (6%)
  other arithmetic  12 us (5%)
    all_to_all x1, waiting for transfers between devices, route_experts(): lax.all_to_all(outgoing, 'ep', split_axis=0, concat_axis=0, tiled=True)  93 us
    all_gather x1, waiting for transfers between devices, route_experts(): lax.all_gather(hidden, 'tp', axis=1, tiled=True)  15.4 us
    all_to_all x1, waiting for transfers between devices, route_experts(): lax.all_to_all(result, 'ep', split_axis=0, concat_axis=0, tiled=True)  9.19 us
    all_gather x1, waiting for transfers between devices, attend(): value_piece = lax.all_gather(values, 'ep', axis=0, tiled=True)  8.72 us
    all_gather x1, waiting for transfers between devices, attend(): lax.all_gather(head_rows, 'tp', axis=1, tiled=True)  7.88 us
    all_to_all x1, starting transfers between devices, route_experts(): lax.all_to_all(outgoing, 'ep', split_axis=0, concat_axis=0, tiled=True)  7.43 us
    dot_general x1, matrix products, attend(): jnp.einsum('qhcd,khcd->cqhk', queries, key_piece, preferred_element_type=...  6.69 us
    all_to_all x1, starting transfers between devices, route_experts(): lax.all_to_all(result, 'ep', split_axis=0, concat_axis=0, tiled=True)  5.51 us
  transfers between devices with their start and end apart: 6, of which 5 were waited for; matrix products, arithmetic and copies ran while one was open for 24% of the time, Pallas kernels for 0%

commit v1 on v0

--- a/solution.py
+++ b/solution.py
@@ -2,6 +2,7 @@
 import jax.numpy as jnp
 from jax import lax
 from jax.sharding import PartitionSpec as P
+from jax.lax import all_gather
 
 
 def rms_rows(matrix, gain, epsilon):
@@ -38,8 +39,9 @@
     )
     values = jnp.dot(normed, w_value, preferred_element_type=jnp.float32).astype(jnp.bfloat16)
     query_pos = lax.axis_index("ep") * row_count + lax.iota(jnp.int32, row_count)
-    key_piece = lax.all_gather(key_rows, "ep", axis=0, tiled=True)
-    value_piece = lax.all_gather(values, "ep", axis=0, tiled=True)
+    reached = jnp.concatenate([key_rows, values], 1)
+    val2 = all_gather(reached, "ep", tiled=True, axis=0)
+    key_piece, value_piece = jnp.split(val2, [key_rows.shape[1]], 1)
     piece_rows = key_piece.shape[0]
     key_piece = key_piece.reshape(piece_rows, head_count, 2, head_size)
     value_piece = value_piece.reshape(piece_rows, head_count, 2 * head_size)

time: 234 us -> 227 us (0.970)
  blocking collectives: 0 us -> 119 us
  waiting for transfers between devices: 134 us -> 18.4 us
  starting transfers between devices: 13.3 us -> 5.81 us
  matrix products: 35.2 us -> 29.1 us
  local copies, waits for them, and re-layouts: 24.7 us -> 29.8 us
    all_to_all x0 -> x1, blocking collectives: none -> 119 us  [route_experts(): lax.all_to_all(outgoing, 'ep', split_axis=0, concat_axis=0, tiled=True)]
    all_to_all x1 -> x0, waiting for transfers between devices: 93 us -> none  [route_experts(): lax.all_to_all(outgoing, 'ep', split_axis=0, concat_axis=0, tiled=True)]
    all_gather x1, waiting for transfers between devices: 15.4 us -> 1.22 us  [route_experts(): lax.all_gather(hidden, 'tp', axis=1, tiled=True)]
    split x0 -> x2, local copies, waits for them, and re-layouts: none -> 8.96 us  [attend(): key_piece, value_piece = jnp.split(val2, [key_rows.shape[1]], 1)]
    all_gather x2 -> x1, waiting for transfers between devices: 8.75 us -> 0.02 us  [attend(): val2 = all_gather(reached, 'ep', tiled=True, axis=0)]
    all_to_all x1 -> x0, starting transfers between devices: 7.43 us -> none  [route_experts(): lax.all_to_all(outgoing, 'ep', split_axis=0, concat_axis=0, tiled=True)]
    all_gather x1 -> x0, local copies, waits for them, and re-layouts: 4 us -> none  [attend(): key_piece = lax.all_gather(key_rows, 'ep', axis=0, tiled=True)]
  transfers between devices with their start and end apart: 6 -> 4, of which waited for: 5 -> 3; matrix products, arithmetic and copies ran while one was open for 24% -> 24% of each run, Pallas kernels for 0% -> 0%
where the time goes in v1:
time: 227 us; the launch traced here: 226 us
  blocking collectives  119 us (52%)
  local copies, waits for them, and re-layouts  29.8 us (13%)
  matrix products  29.1 us (13%)
  waiting for transfers between devices  18.4 us (8%)
  between operations  14.1 us (6%)
  other arithmetic  10.4 us (5%)
  starting transfers between devices  5.81 us (3%)
    all_to_all x1, blocking collectives, route_experts(): lax.all_to_all(outgoing, 'ep', split_axis=0, concat_axis=0, tiled=True)  119 us
    all_to_all x1, waiting for transfers between devices, route_experts(): lax.all_to_all(result, 'ep', split_axis=0, concat_axis=0, tiled=True)  9.09 us
    split x2, local copies, waits for them, and re-layouts, attend(): key_piece, value_piece = jnp.split(val2, [key_rows.shape[1]], 1)  8.96 us
    all_gather x1, waiting for transfers between devices, attend(): lax.all_gather(head_rows, 'tp', axis=1, tiled=True)  7.99 us
    dot_general x1, matrix products, attend(): jnp.einsum('qhcd,khcd->cqhk', queries, key_piece, preferred_element_type=...  6.69 us
    all_to_all x1, starting transfers between devices, route_experts(): lax.all_to_all(result, 'ep', split_axis=0, concat_axis=0, tiled=True)  5.51 us
    dot_general x1, matrix products, route_experts(): jnp.dot(lax.all_gather(hidden, 'tp', axis=1, tiled=True), down_local, pre...  5.25 us
  transfers between devices with their start and end apart: 4, of which 3 were waited for; matrix products, arithmetic and copies ran while one was open for 24% of the time, Pallas kernels for 0%

profile of v1, /device:TPU:0, one launch (start us, length us, event | category | flops | bytes accessed | tf_op | source)
XLA Modules:
  0.0 226.5 jit_solution(13190883813159320639)
XLA Ops:
  7.2 1.6 fusion.4
  8.9 2.8 %convolution_convert_fusion.1 = bf16[256,512]{1,0:T(8,128)(2,1)S(1)} fusion(bf16[2048,512]{1,0:T(8,128)(2,1)} %param.21, bf16[256,2048]{1,0:T(8,128)(2,1)} %param.17, f32[2048]{0:T(1024)} %param.18, f32[256]{0:T(256)S(1)} %add_rsqrt_fusion.3), kind=kOutput, calls=%fused_computation.30 | convolution fusion | flops 539099136 | bytes 3417088 | tf_op jit(solution)/shard_map/dot_general | solution.py:40
  11.8 1.5 fusion.53
  13.6 0.9 mul.193
  14.5 1.3 copy.27
  15.9 1.1 multiply_convert_fusion.2
  17.0 0.9 pad_maximum_fusion
  18.8 1.1 reduce-window.6
  20.3 2.4 %scatter_custom_fusion.1 = s32[768]{0:T(1024)S(1)} fusion(s32[512]{0:T(512)S(1)} %bitcast.125, s32[512]{0:T(512)S(1)} %add_select_fusion, s32[]{:T(128)} %constant.65.clone.1), kind=kCustom, calls=%fused_computation.77 | custom fusion | bytes 3076 | tf_op jit(solution)/shard_map/scatter | solution.py:87
  22.8 2.4 %scatter_custom_fusion = pred[768]{0:T(1024)(128)(4,1)S(1)} fusion(s32[512]{0:T(512)S(1)} %bitcast.126, pred[512]{0:T(512)(128)(4,1)S(1)} %broadcast.164, pred[]{:T(512)} %constant.25.clone.1), kind=kCustom, calls=%fused_computation.80 | custom fusion | bytes 769 | tf_op jit(solution)/shard_map/scatter | solution.py:88
  25.5 4.3 %gather_fusion = bf16[768,2048]{1,0:T(8,128)(2,1)} fusion(bf16[128,2048]{1,0:T(8,128)(2,1)S(1)} %fusion.25, s32[1024]{0:T(1024)S(1)} %pad_clamp_fusion.1), kind=kCustom, calls=%fused_computation | custom fusion | bytes 6294528 | tf_op jit(solution)/shard_map/gather | solution.py:89
  29.8 2.2 broadcast_select_fusion
  32.0 118.9 %all_to_all.10 = bf16[8,96,2048]{2,1,0:T(8,128)(2,1)S(1)} all-to-all(bf16[8,96,2048]{2,1,0:T(8,128)(2,1)S(1)} %broadcast_select_fusion), channel_id=1, replica_groups=mesh['ep'=8,'tp'=4] {'ep'}, dimensions={0} | all-to-all | bytes 6291456 | tf_op jit(solution)/shard_map/all_to_all | solution.py:91
  150.9 1.8 fusion.11
  152.7 3.0 %multiply_convert_fusion = bf16[768,512]{1,0:T(8,128)(2,1)} fusion(f32[768,512]{1,0:T(8,128)S(1)} %fusion.11, bf16[768,2048]{1,0:T(8,128)(2,1)S(1)} %bitcast.120, bf16[1,2048,512]{2,1,0:T(8,128)(2,1)S(1)} %copy-done.12), kind=kOutput, calls=%fused_computation.24 | convolution fusion | flops 1614544896 | bytes 7602176 | tf_op jit(solution)/shard_map/dot_general | solution.py:95
  156.1 3.4 %multiply_reduce_fusion.1 = (f32[256,4,2]{0,2,1:T(2,128)S(1)}, f32[256,512]{0,1:T(8,128)}) fusion(bf16[2048,512]{1,0:T(8,128)(2,1)} %param.19, bf16[256,2048]{1,0:T(8,128)(2,1)S(1)} %copy-done.4, f32[2048]{0:T(1024)S(1)} %copy-done.13, f32[256]{0:T(256)S(1)} %add_rsqrt_fusion.3), kind=kOutput, calls=%fused_computation.50 | convolution fusion | flops 539228160 | bytes 3687424 | tf_op jit(solution)/shard_map/dot_general | solution.py:28
  159.5 0.3 iota_compare_fusion
  159.9 4.9 %fusion.51 = (bf16[2048,512]{1,0:T(8,128)(2,1)}, bf16[2048,512]{1,0:T(8,128)(2,1)}) fusion(bf16[2048,1024]{1,0:T(8,128)(2,1)} %all-gather.4.cloned.1.call-done), kind=kLoop, calls=%fused_computation.90 | loop fusion | bytes 8388608 | tf_op jit(solution)/shard_map/split | solution.py:44
  164.8 4.0 %copy.42 = bf16[2048,512]{0,1:T(8,128)(2,1)} copy(bf16[2048,512]{1,0:T(8,128)(2,1)} %get-tuple-element.5) | data formatting | bytes 4194304 | tf_op jit(solution)/shard_map/reshape | solution.py:47
  168.8 4.0 %copy.28 = bf16[2048,512]{0,1:T(8,128)(2,1)} copy(bf16[2048,512]{1,0:T(8,128)(2,1)} %get-tuple-element.4) | data formatting | bytes 4194304 | tf_op jit(solution)/shard_map/split | solution.py:44
  172.8 6.7 %fusion = (f32[2,256,4]{1,2,0:T(4,128)S(1)}, bf16[2,256,4,2048]{1,3,2,0:T(8,128)(2,1)S(1)}) fusion(pred[256,2048]{0,1:T(8,128)(4,1)S(1)} %iota_compare_fusion, bf16[2048,4,2,64]{0,3,2,1:T(8,128)(2,1)} %bitcast.122, f32[64]{0:T(128)S(1)} %copy-done.14, f32[256,4,2]{0,2,1:T(2,128)S(1)} %add_rsqrt_fusion, f32[256,512]{0,1:T(8,128)S(1)} %copy-done.15), kind=kOutput, calls=%fused_computation.5 | convolution fusion | flops 549976064 | bytes 11550976 | tf_op jit(solution)/shard_map/qhcd,khcd->cqhk/dot_general | solution.py:48
  179.6 1.3 fusion.20
  181.1 0.9 fusion.33
  182.1 1.2 all-gather.8.cloned.1.call-done
  183.3 5.2 %fusion.17 = bf16[768,512]{1,0:T(8,128)(2,1)} fusion(bf16[768,2048]{1,0:T(8,128)(2,1)} %all-gather.8.cloned.1.call-done, bf16[1,2048,512]{2,1,0:T(8,128)(2,1)} %param.33), kind=kOutput, calls=%fused_computation.25 | convolution fusion | flops 1611005952 | bytes 6029312 | tf_op jit(solution)/shard_map/dot_general | solution.py:103
  188.5 5.5 %all-to-all-start.1 = ((bf16[8,96,512]{2,1,0:T(8,128)(2,1)}), bf16[8,96,512]{2,1,0:T(8,128)(2,1)S(1)}, u32[]{:S(2)}, u32[]{:S(2)}) async-start(bf16[8,96,512]{2,1,0:T(8,128)(2,1)} %bitcast.124), calls=%async_computation.1 | async-start | bytes 1572864 | tf_op jit(solution)/shard_map/all_to_all | solution.py:109
  194.2 8.0 %all-gather.6.cloned.1.call-done = bf16[256,2048]{0,1:T(8,128)(2,1)} async-done(((bf16[256,512]{0,1:T(8,128)(2,1)}), bf16[256,2048]{0,1:T(8,128)(2,1)}) %all-gather.6.cloned.1.call-update) | async-done | bytes 1048592 | tf_op jit(solution)/shard_map/all_gather | solution.py:67
  202.2 3.3 %convolution_convert_fusion = bf16[256,512]{1,0:T(8,128)(2,1)} fusion(bf16[256,2048]{0,1:T(8,128)(2,1)} %all-gather.6.cloned.1.call-done, bf16[2048,512]{1,0:T(8,128)(2,1)} %param.26), kind=kOutput, calls=%fused_computation.29 | convolution fusion | flops 537001984 | bytes 3407872 | tf_op jit(solution)/shard_map/dot_general | solution.py:66
  205.5 9.1 %all-to-all-done.1 = bf16[8,96,512]{2,1,0:T(8,128)(2,1)S(1)} async-done(((bf16[8,96,512]{2,1,0:T(8,128)(2,1)}), bf16[8,96,512]{2,1,0:T(8,128)(2,1)S(1)}, u32[]{:S(2)}, u32[]{:S(2)}) %all-to-all-start.1) | async-done | bytes 786464 | tf_op jit(solution)/shard_map/all_to_all | solution.py:109
  214.6 2.6 %gather_fusion.1 = bf16[512,512]{1,0:T(8,128)(2,1)} fusion(bf16[768,512]{1,0:T(8,128)(2,1)S(1)} %bitcast.117, s32[1024]{0:T(1024)S(1)} %pad_clamp_fusion), kind=kCustom, calls=%fused_computation.1 | custom fusion | bytes 1050624 | tf_op jit(solution)/shard_map/gather | solution.py:110
  217.2 1.4 reshape.170
  218.6 1.4 multiply_reduce_fusion
  (74 shorter events, 2.7 us)
Async XLA Ops:
  7.2 143.7 %copy-start = (bf16[1,2048,512]{2,1,0:T(8,128)(2,1)S(1)}, bf16[1,2048,512]{2,1,0:T(8,128)(2,1)}, u32[]{:S(2)}) copy-start(bf16[1,2048,512]{2,1,0:T(8,128)(2,1)} %param.31) | copy-start | bytes 6291460
  7.2 152.7 %all-gather.4.cloned.1.call-start = ((), (), s32[]{:S(2)}) async-start(), calls=%async_computation.2 | async-start | bytes 4718592 | tf_op jit(solution)/shard_map/all_gather | solution.py:43
  8.9 2.9 %copy-start.3 = (bf16[256,2048]{1,0:T(8,128)(2,1)S(1)}, bf16[256,2048]{1,0:T(8,128)(2,1)}, u32[]{:S(2)}) copy-start(bf16[256,2048]{1,0:T(8,128)(2,1)} %param.17) | copy-start | bytes 3145732
  8.9 2.9 %copy-start.11 = (bf16[2048,512]{1,0:T(8,128)(2,1)S(1)}, bf16[2048,512]{1,0:T(8,128)(2,1)}, u32[]{:S(2)}) copy-start(bf16[2048,512]{1,0:T(8,128)(2,1)} %param.20) | copy-start | bytes 6291460
  8.9 2.9 %copy-start.13 = (f32[2048]{0:T(1024)S(1)}, f32[2048]{0:T(1024)}, u32[]{:S(2)}) copy-start(f32[2048]{0:T(1024)} %param.18) | copy-start | bytes 24580
  13.3 2.4 %copy-start.9 = (f32[64]{0:T(128)S(1)}, f32[64]{0:T(128)}, u32[]{:S(2)}) copy-start(f32[64]{0:T(128)} %param.23) | copy-start | bytes 772
  14.5 3.5 %copy-start.6 = (s32[128,4]{0,1:T(4,128)S(1)}, s32[128,4]{0,1:T(4,128)}, u32[]{:S(2)}) copy-start(s32[128,4]{0,1:T(4,128)} %param.29) | copy-start | bytes 6148
  14.5 3.9 %copy-start.2 = (bf16[128,2048]{1,0:T(8,128)(2,1)S(1)}, bf16[128,2048]{1,0:T(8,128)(2,1)}, u32[]{:S(2)}) copy-start(bf16[128,2048]{1,0:T(8,128)(2,1)} %param.27) | copy-start | bytes 1572868
  15.8 9.5 %copy-start.5 = (f32[2048]{0:T(1024)S(1)}, f32[2048]{0:T(1024)}, u32[]{:S(2)}) copy-start(f32[2048]{0:T(1024)} %param.28) | copy-start | bytes 24580
  17.9 165.4 %all-gather.8.cloned.1.call-start = ((), (), s32[]{:S(2)}) async-start(), calls=%async_computation.4 | async-start | bytes 3932160 | tf_op jit(solution)/shard_map/all_gather | solution.py:104
  150.9 1.8 copy-start.12
  152.7 3.3 %copy-start.7 = (f32[4]{0:T(128)S(1)}, f32[4]{0:T(128)}, u32[]{:S(2)}) copy-start(f32[4]{0:T(128)} %param.24) | copy-start | bytes 52
  152.7 3.3 %copy-start.10 = (f32[128]{0:T(128)S(1)}, f32[128]{0:T(128)}, u32[]{:S(2)}) copy-start(f32[128]{0:T(128)} %param.25) | copy-start | bytes 1540
  152.7 3.4 %copy-start.4 = (bf16[256,2048]{1,0:T(8,128)(2,1)S(1)}, bf16[256,2048]{1,0:T(8,128)(2,1)}, u32[]{:S(2)}) copy-start(bf16[256,2048]{1,0:T(8,128)(2,1)} %param.17) | copy-start | bytes 3145732
  155.7 46.4 %all-gather.6.cloned.1.call-start = ((), (), s32[]{:S(2)}) async-start(), calls=%async_computation.3 | async-start | bytes 1310720 | tf_op jit(solution)/shard_map/all_gather | solution.py:67
  168.8 4.0 %copy-start.14 = (f32[64]{0:T(128)S(1)}, f32[64]{0:T(128)}, u32[]{:S(2)}) copy-start(f32[64]{0:T(128)} %param.22) | copy-start | bytes 772
  168.8 4.0 %copy-start.15 = (f32[256,512]{0,1:T(8,128)S(1)}, f32[256,512]{0,1:T(8,128)}, u32[]{:S(2)}) copy-start(f32[256,512]{0,1:T(8,128)} %get-tuple-element.13) | copy-start | bytes 1572868
  172.8 6.7 %copy-start.1 = (bf16[2048,512]{0,1:T(8,128)(2,1)S(1)}, bf16[2048,512]{0,1:T(8,128)(2,1)}, u32[]{:S(2)}) copy-start(bf16[2048,512]{0,1:T(8,128)(2,1)} %copy.42) | copy-start | bytes 6291460
  182.1 12.0 %copy-start.8 = (f32[128,4]{0,1:T(4,128)S(1)}, f32[128,4]{0,1:T(4,128)}, u32[]{:S(2)}) copy-start(f32[128,4]{0,1:T(4,128)} %param.30) | copy-start | bytes 6148
  188.5 26.1 %all-to-all-start.1 = ((bf16[8,96,512]{2,1,0:T(8,128)(2,1)}), bf16[8,96,512]{2,1,0:T(8,128)(2,1)S(1)}, u32[]{:S(2)}, u32[]{:S(2)}) async-start(bf16[8,96,512]{2,1,0:T(8,128)(2,1)} %bitcast.124), calls=%async_computation.1 | async-start | bytes 1572864 | tf_op jit(solution)/shard_map/all_to_all | solution.py:109
Sparse Core Ops, SparseCore 0:
  18.0 123.4 all-gather.3
  155.9 27.3 all-gather.7
  185.4 16.6 all-gather.5
